TPU v7x, 512 devices: a whole 4x8x8 slice. The times are simulated.
512 devices in a mesh: row: 64 (over z, y), col: 8 (over x, core).
Axes of the slice: x: 4, y: 8, z: 8, core: 2. Of those that a mesh axis runs over, the one named last changes fastest.
Arguments:
- tokens: bfloat16 [8, 24576, 2048], P('col', 'row'), may hold values from -6 to 6
- norm_gain: bfloat16 [2048], replicated, may hold values from 0.099609375 to 1.8984375
- in_weight: bfloat16 [2048, 512], P('row', 'col'), may hold values from -0.125 to 0.125
- out_weight: bfloat16 [512, 2048], P('col', 'row'), may hold values from -0.25 to 0.25
Outputs:
- mixed: bfloat16 [8, 24576, 2048], P('col', 'row')
All inputs are finite; a program needn't handle non-finite values.
Results may differ from a plain program's by a relative error of at most 0.013.
Values may be sent and summed in bfloat16 or wider, within the bound.
A program may use at most 64 MiB of HBM per device.

v0:
```python
import math
import jax
import jax.numpy as jnp
from jax import lax
from jax.sharding import Mesh
from jax.sharding import PartitionSpec as P

GS = 64
ROW = ("row_0", "row_1")
EPS = 1e-06


def turned_gather(arrays, axis, dims):
    turned = [jnp.moveaxis(a, dim, 0) for a, dim in zip(arrays, dims)]
    widths = [t[0].size for t in turned]
    both = jnp.concatenate([t.reshape(-1, w) for t, w in zip(turned, widths)], axis=1)
    out = lax.all_gather(both, axis, axis=0, tiled=True)
    pieces = jnp.split(out, [sum(widths[:k]) for k in range(1, len(widths))], axis=1)
    return tuple(
        (
            jnp.moveaxis(b.reshape(-1, *t.shape[1:]), 0, dim)
            for b, t, dim in zip(pieces, turned, dims)
        )
    )


def joined_along(pieces, dim):
    pieces = jnp.moveaxis(pieces, 0, dim)
    lengths = pieces.shape
    return pieces.reshape(*lengths[:dim], lengths[dim] * lengths[dim + 1], *lengths[dim + 2 :])


def all_blocks(shard, axes, sequence):
    pieces = shard
    for k in sequence:
        pieces = lax.all_gather(pieces, axes[k])
    done = sequence[::-1]
    back = [done.index(k) for k in range(len(axes))]
    pieces = pieces.transpose(*back, *range(len(axes), pieces.ndim))
    return pieces.reshape(-1, *shard.shape)


def gather_axes(shard, axes, sequence, dim):
    return joined_along(all_blocks(shard, axes, sequence), dim)


def angle_pair(left_index, right_index, modulus):
    product = left_index[:, None] * right_index[None, :] % modulus
    radians = product.astype(jnp.float32) * (2.0 * math.pi / modulus)
    return (jnp.cos(radians), jnp.sin(radians))


def table_dot(matrix, values):
    return jnp.dot(matrix, values, preferred_element_type=jnp.float32)


def right_dot(values, matrix):
    return jnp.dot(values, matrix, preferred_element_type=jnp.float32)


def body(tokens, norm_gain, in_weight, out_weight):
    own_rows = tokens[0].astype(jnp.float32)
    inverse_rms = lax.rsqrt(jnp.mean(own_rows * own_rows, axis=-1, keepdims=True) + EPS)
    normed = (own_rows * inverse_rms * norm_gain.astype(jnp.float32)).astype(jnp.bfloat16)
    in_columns, out_rows = turned_gather((in_weight, out_weight), "col", (1, 0))
    row_count = normed.shape[0]
    channels = in_columns.shape[1]
    peer_count = lax.axis_size(ROW)
    length = row_count * peer_count
    projected = jnp.dot(
        normed, gather_axes(in_columns, ROW, (0, 1), 0), preferred_element_type=jnp.float32
    ).astype(jnp.bfloat16)
    channel_index = jnp.arange(channels, dtype=jnp.int32)
    within = channel_index % GS
    same_group = channel_index[:, None] // GS == channel_index[None, :] // GS
    group_cos, group_sin = angle_pair(within, within, GS)
    group_cos = jnp.where(same_group, group_cos, 0.0)
    group_sin = jnp.where(same_group, group_sin, 0.0)
    peer_index = jnp.arange(peer_count, dtype=jnp.int32)
    small_cos, small_sin = angle_pair(peer_index, peer_index, peer_count)
    line_index = jnp.arange(row_count, dtype=jnp.int32)
    long_cos, long_sin = angle_pair(line_index, line_index, row_count)
    gathered = lax.all_to_all(projected, ROW, split_axis=1, concat_axis=0, tiled=True).astype(
        jnp.float32
    )
    narrow = gathered.shape[1]
    flat = gathered.reshape(peer_count, row_count * narrow)
    first_real = table_dot(small_cos, flat).reshape(peer_count, row_count, narrow)
    first_imag = (-table_dot(small_sin, flat)).reshape(peer_count, row_count, narrow)
    turn_cos, turn_sin = angle_pair(peer_index, line_index, length)
    turn_cos = turn_cos[:, :, None]
    turn_sin = turn_sin[:, :, None]
    turned_real = first_real * turn_cos + first_imag * turn_sin
    turned_imag = first_imag * turn_cos - first_real * turn_sin
    lines_real = turned_real.transpose(1, 0, 2).reshape(row_count, peer_count * narrow)
    lines_imag = turned_imag.transpose(1, 0, 2).reshape(row_count, peer_count * narrow)
    whole_real = (table_dot(long_cos, lines_real) + table_dot(long_sin, lines_imag)).reshape(
        length, narrow
    )
    whole_imag = (table_dot(long_cos, lines_imag) - table_dot(long_sin, lines_real)).reshape(
        length, narrow
    )
    back_real, back_imag = (
        lax.all_to_all(
            whole_real.astype(jnp.bfloat16), ROW, split_axis=0, concat_axis=1, tiled=True
        ).astype(whole_real.dtype),
        lax.all_to_all(
            whole_imag.astype(jnp.bfloat16), ROW, split_axis=0, concat_axis=1, tiled=True
        ).astype(whole_imag.dtype),
    )
    mixed_real = right_dot(back_real, group_cos) + right_dot(back_imag, group_sin)
    arranged = (mixed_real * (1.0 / math.sqrt(length * GS))).astype(jnp.bfloat16)
    result = jnp.dot(
        arranged,
        lax.all_gather(out_rows, ROW, axis=1, tiled=True),
        preferred_element_type=jnp.float32,
    )
    return result.astype(jnp.bfloat16)[None]


def solution(mesh):
    split = Mesh(mesh.devices.reshape(8, 8, mesh.shape["col"]), ("row_0", "row_1", "col"))
    in_specs = (P("col", ROW, None), P(), P(ROW, "col"), P("col", ROW))
    out_specs = P("col", ROW, None)
    return jax.shard_map(body, mesh=split, in_specs=in_specs, out_specs=out_specs, check_vma=False)
```

profile of v0, /device:TPU:2, one launch (start us, length us, event | category | flops | bytes accessed | tf_op | source)
XLA Modules:
  0.0 213.6 jit_solution(14317200805764714633)
XLA Ops:
  6.5 0.0 copy-start
  6.5 0.0 all-gather.7.cloned.1.call-start
  6.5 0.9 copy.54
  7.4 0.8 copy.55
  8.2 0.1 pad_maximum_fusion
  8.3 15.4 %all_gather.18 = bf16[512,64]{1,0:T(8,128)(2,1)S(1)} all-gather(bf16[64,64]{1,0:T(8,128)(2,1)S(1)} %pad_maximum_fusion), channel_id=1, replica_groups=mesh['row_0'=8,'row_1'=8,'col'=8] {'col'}, dimensions={0}, use_global_device_ids=true | all-gather | bytes 73728 | tf_op jit(solution)/shard_map/all_gather | solution.py:17
  23.8 0.1 fusion.135
  23.9 0.1 copy.70
  24.0 30.5 %all-gather = bf16[256,512]{1,0:T(8,128)(2,1)} all-gather(bf16[32,512]{1,0:T(8,128)(2,1)S(1)} %bitcast.62), channel_id=2, replica_groups=mesh['row_0'=8,'row_1'=8,'col'=8] {'row_0'}, dimensions={0}, use_global_device_ids=true | all-gather | bytes 294912 | tf_op jit(solution)/shard_map/all_gather | solution.py:36
  54.5 0.0 all-gather.7.cloned.1.call-update
  54.5 0.0 all-gather.5.cloned.1.call-start
  54.5 0.7 copy.68
  55.2 0.0 all-gather.5.cloned.1.call-update
  55.3 0.7 convert_element_type.78
  55.9 0.0 copy-done
  56.0 0.4 fusion
  56.3 39.7 %all-gather.7.cloned.1.call-done = bf16[64,32,512]{2,1,0:T(8,128)(2,1)} async-done(((bf16[8,32,512]{2,1,0:T(8,128)(2,1)}), bf16[64,32,512]{2,1,0:T(8,128)(2,1)}) %all-gather.7.cloned.1.call-update) | async-done | bytes 2097168 | tf_op jit(solution)/shard_map/all_gather | solution.py:36
  96.0 1.8 copy.57
  97.9 1.0 fusion.13
  98.9 0.9 copy.58
  99.8 10.7 %all-to-all-start = ((bf16[384,64,8]{0,2,1:T(8,128)(2,1)}), bf16[384,64,8]{0,2,1:T(8,128)(2,1)S(1)}, u32[]{:S(2)}, u32[]{:S(2)}) async-start(bf16[384,64,8]{0,2,1:T(8,128)(2,1)} %bitcast.8), calls=%async_computation | async-start | bytes 786432 | tf_op jit(solution)/shard_map/all_to_all | solution.py:83
  110.6 0.4 fusion.78
  111.0 14.1 %all-to-all-done = bf16[384,64,8]{0,2,1:T(8,128)(2,1)S(1)} async-done(((bf16[384,64,8]{0,2,1:T(8,128)(2,1)}), bf16[384,64,8]{0,2,1:T(8,128)(2,1)S(1)}, u32[]{:S(2)}, u32[]{:S(2)}) %all-to-all-start) | async-done | bytes 393248 | tf_op jit(solution)/shard_map/all_to_all | solution.py:83
  125.1 0.6 copy.59
  125.7 0.5 convolution_negate_fusion
  126.2 0.5 copy.61
  126.7 0.5 copy.62
  127.2 0.5 subtract_bitcast_fusion
  127.7 2.5 %fusion.26 = f32[384,512]{1,0:T(8,128)S(1)} fusion(bf16[384,64,8]{0,1,2:T(8,128)(2,1)S(1)} %get-tuple-element.6), kind=kOutput, calls=%fused_computation.38 | convolution fusion | flops 152322048 | bytes 1179648 | tf_op jit(solution)/shard_map/dot_general | solution.py:54
  130.2 2.9 %fusion.10 = bf16[384,512]{1,0:T(8,128)(2,1)S(1)} fusion(f32[384,512]{1,0:T(8,128)S(1)} %fusion.26, bf16[384,64,8]{0,1,2:T(8,128)(2,1)S(1)} %get-tuple-element.5), kind=kOutput, calls=%fused_computation.23 | convolution fusion | flops 152715264 | bytes 1572864 | tf_op jit(solution)/shard_map/dot_general | solution.py:54
  133.1 8.4 %convert_element_type.84 = bf16[64,384,8]{2,1,0:T(8,128)(2,1)} reshape(bf16[384,512]{1,0:T(8,128)(2,1)S(1)} %fusion.10) | data formatting | bytes 786432 | tf_op jit(solution)/shard_map/convert_element_type | solution.py:105
  141.5 5.8 %copy.66 = bf16[64,384,8]{1,2,0:T(8,128)(2,1)} copy(bf16[64,384,8]{2,1,0:T(8,128)(2,1)} %convert_element_type.84) | data formatting | bytes 786432 | tf_op jit(solution)/shard_map/convert_element_type | solution.py:105
  147.3 4.8 %all-to-all-start.1 = ((bf16[64,384,8]{1,2,0:T(8,128)(2,1)}), bf16[64,384,8]{1,2,0:T(8,128)(2,1)S(1)}, u32[]{:S(2)}, u32[]{:S(2)}) async-start(bf16[64,384,8]{1,2,0:T(8,128)(2,1)} %copy.66), calls=%async_computation.1 | async-start | bytes 786432 | tf_op jit(solution)/shard_map/all_to_all | solution.py:104
  152.1 2.5 %fusion.22 = f32[384,512]{1,0:T(8,128)S(1)} fusion(bf16[384,64,8]{0,1,2:T(8,128)(2,1)S(1)} %get-tuple-element.5), kind=kOutput, calls=%fused_computation.34 | convolution fusion | flops 152322048 | bytes 1179648 | tf_op jit(solution)/shard_map/dot_general | solution.py:54
  154.6 2.9 %fusion.11 = bf16[384,512]{1,0:T(8,128)(2,1)S(1)} fusion(f32[384,512]{1,0:T(8,128)S(1)} %fusion.22, bf16[384,64,8]{0,1,2:T(8,128)(2,1)S(1)} %get-tuple-element.6), kind=kOutput, calls=%fused_computation.24 | convolution fusion | flops 152715264 | bytes 1572864 | tf_op jit(solution)/shard_map/dot_general | solution.py:54
  157.5 8.4 %convert_element_type.87 = bf16[64,384,8]{2,1,0:T(8,128)(2,1)} reshape(bf16[384,512]{1,0:T(8,128)(2,1)S(1)} %fusion.11) | data formatting | bytes 786432 | tf_op jit(solution)/shard_map/convert_element_type | solution.py:108
  165.9 5.8 %copy.67 = bf16[64,384,8]{1,2,0:T(8,128)(2,1)} copy(bf16[64,384,8]{2,1,0:T(8,128)(2,1)} %convert_element_type.87) | data formatting | bytes 786432 | tf_op jit(solution)/shard_map/convert_element_type | solution.py:108
  171.7 0.0 all-to-all-done.1
  171.7 12.9 %all-to-all-start.2 = ((bf16[64,384,8]{1,2,0:T(8,128)(2,1)}), bf16[64,384,8]{1,2,0:T(8,128)(2,1)S(1)}, u32[]{:S(2)}, u32[]{:S(2)}) async-start(bf16[64,384,8]{1,2,0:T(8,128)(2,1)} %copy.67), calls=%async_computation.2 | async-start | bytes 786432 | tf_op jit(solution)/shard_map/all_to_all | solution.py:107
  184.7 4.2 %fusion.16 = f32[384,512]{1,0:T(8,128)S(1)} fusion(s32[512]{0:T(512)S(1)} %get-tuple-element.11, s32[512]{0:T(512)S(1)} %get-tuple-element.12, bf16[64,384,8]{1,2,0:T(8,128)(2,1)S(1)} %all-to-all-done.1), kind=kOutput, calls=%fused_computation.27 | convolution fusion | flops 205520896 | bytes 1183744 | tf_op jit(solution)/shard_map/dot_general | solution.py:58
  188.8 0.0 all-gather.5.cloned.1.call-done
  188.9 10.1 %all-to-all-done.2 = bf16[64,384,8]{1,2,0:T(8,128)(2,1)S(1)} async-done(((bf16[64,384,8]{1,2,0:T(8,128)(2,1)}), bf16[64,384,8]{1,2,0:T(8,128)(2,1)S(1)}, u32[]{:S(2)}, u32[]{:S(2)}) %all-to-all-start.2) | async-done | bytes 393248 | tf_op jit(solution)/shard_map/all_to_all | solution.py:107
  199.0 7.8 %fusion.3 = bf16[1,384,2048]{2,1,0:T(8,128)(2,1)} fusion(bf16[512,2048]{0,1:T(8,128)(2,1)} %all-gather.5.cloned.1.call-done, f32[384,512]{1,0:T(8,128)S(1)} %fusion.16, s32[512]{0:T(512)S(1)} %get-tuple-element.11, s32[512]{0:T(512)S(1)} %get-tuple-element.12, bf16[64,384,8]{1,2,0:T(8,128)(2,1)S(1)} %all-to-all-done.2), kind=kOutput, calls=%fused_computation.7 | convolution fusion | flops 1012203520 | bytes 4853760 | tf_op jit(solution)/shard_map/dot_general | solution.py:113
  (2 shorter events, 0.0 us)
Async XLA Ops:
  6.5 49.4 %copy-start = (bf16[1,384,2048]{2,1,0:T(8,128)(2,1)S(1)}, bf16[1,384,2048]{2,1,0:T(8,128)(2,1)}, u32[]{:S(2)}) copy-start(bf16[1,384,2048]{2,1,0:T(8,128)(2,1)} %param.4) | copy-start | bytes 4718596
  6.5 89.5 %all-gather.7.cloned.1.call-start = ((), (), s32[]{:S(2)}) async-start(), calls=%async_computation.4 | async-start | bytes 2359296 | tf_op jit(solution)/shard_map/all_gather | solution.py:36
  54.5 134.4 %all-gather.5.cloned.1.call-start = ((), (), s32[]{:S(2)}) async-start(), calls=%async_computation.3 | async-start | bytes 2129920 | tf_op jit(solution)/shard_map/all_gather | solution.py:115
  99.8 25.3 %all-to-all-start = ((bf16[384,64,8]{0,2,1:T(8,128)(2,1)}), bf16[384,64,8]{0,2,1:T(8,128)(2,1)S(1)}, u32[]{:S(2)}, u32[]{:S(2)}) async-start(bf16[384,64,8]{0,2,1:T(8,128)(2,1)} %bitcast.8), calls=%async_computation | async-start | bytes 786432 | tf_op jit(solution)/shard_map/all_to_all | solution.py:83
  147.3 24.4 %all-to-all-start.1 = ((bf16[64,384,8]{1,2,0:T(8,128)(2,1)}), bf16[64,384,8]{1,2,0:T(8,128)(2,1)S(1)}, u32[]{:S(2)}, u32[]{:S(2)}) async-start(bf16[64,384,8]{1,2,0:T(8,128)(2,1)} %copy.66), calls=%async_computation.1 | async-start | bytes 786432 | tf_op jit(solution)/shard_map/all_to_all | solution.py:104
  171.7 27.3 %all-to-all-start.2 = ((bf16[64,384,8]{1,2,0:T(8,128)(2,1)}), bf16[64,384,8]{1,2,0:T(8,128)(2,1)S(1)}, u32[]{:S(2)}, u32[]{:S(2)}) async-start(bf16[64,384,8]{1,2,0:T(8,128)(2,1)} %copy.67), calls=%async_computation.2 | async-start | bytes 786432 | tf_op jit(solution)/shard_map/all_to_all | solution.py:107
Sparse Core Ops, SparseCore 0:
  54.6 41.3 all-gather.6
  99.1 85.8 all-gather.4
where the time goes:
time: 214 us
  waiting for transfers between devices  64 us (30%)
  blocking collectives  45.9 us (21%)
  local copies, waits for them, and re-layouts  35.3 us (16%)
  starting transfers between devices  28.5 us (13%)
  matrix products  24.7 us (12%)
  between operations  13.5 us (6%)
    all_gather x1, waiting for transfers between devices, all_blocks(): pieces = lax.all_gather(pieces, axes[k])  39.7 us
    all_gather x1, blocking collectives, all_blocks(): pieces = lax.all_gather(pieces, axes[k])  30.5 us
    all_gather x1, blocking collectives, turned_gather(): out = lax.all_gather(both, axis, axis=0, tiled=True)  15.4 us
    convert_element_type x2, local copies, waits for them, and re-layouts, body(): whole_imag.astype(jnp.bfloat16)  14.2 us
    convert_element_type x2, local copies, waits for them, and re-layouts, body(): whole_real.astype(jnp.bfloat16)  14.2 us
    all_to_all x1, waiting for transfers between devices, body(): lax.all_to_all(projected, ROW, split_axis=1, concat_axis=0, tiled=True)  14.1 us
    all_to_all x1, starting transfers between devices, body(): lax.all_to_all(whole_imag.astype(jnp.bfloat16), ROW, split_axis=0, concat...  12.9 us
    dot_general x6, matrix products, table_dot(): return jnp.dot(matrix, values, preferred_element_type=jnp.float32)  11.7 us
  transfers between devices with their start and end apart: 5, of which 3 were waited for; matrix products, arithmetic and copies ran while one was open for 24% of the time, Pallas kernels for 0%

commit v1 on v0

--- a/solution.py
+++ b/solution.py
@@ -14,7 +14,9 @@
     turned = [jnp.moveaxis(a, dim, 0) for a, dim in zip(arrays, dims)]
     widths = [t[0].size for t in turned]
     both = jnp.concatenate([t.reshape(-1, w) for t, w in zip(turned, widths)], axis=1)
-    out = lax.all_gather(both, axis, axis=0, tiled=True)
+    out = jnp.concatenate(
+        lax.all_to_all(jnp.stack([both] * lax.axis_size(axis)), axis, 0, 0), axis=0
+    )
     pieces = jnp.split(out, [sum(widths[:k]) for k in range(1, len(widths))], axis=1)
     return tuple(
         (

time: 214 us -> 210 us (0.981)
  blocking collectives: 45.9 us -> 42 us
    all_gather x1 -> x0, blocking collectives: 15.4 us -> none  [turned_gather(): out = lax.all_gather(both, axis, axis=0, tiled=True)]
    all_to_all x0 -> x1, blocking collectives: none -> 12.4 us  [turned_gather(): lax.all_to_all(jnp.stack([both] * lax.axis_size(axis)), axis, 0, 0)]
  transfers between devices with their start and end apart: 5 -> 5, of which waited for: 3 -> 3; matrix products, arithmetic and copies ran while one was open for 24% -> 25% of each run, Pallas kernels for 0% -> 0%
where the time goes in v1:
time: 210 us; the launch traced here: 209 us
  waiting for transfers between devices  64.2 us (31%)
  blocking collectives  42 us (20%)
  local copies, waits for them, and re-layouts  33.9 us (16%)
  starting transfers between devices  28.3 us (13%)
  matrix products  24.7 us (12%)
  between operations  13.5 us (6%)
  other arithmetic  2.34 us (1%)
    all_gather x1, waiting for transfers between devices, all_blocks(): pieces = lax.all_gather(pieces, axes[k])  39.6 us
    all_gather x1, blocking collectives, all_blocks(): pieces = lax.all_gather(pieces, axes[k])  29.6 us
    convert_element_type x2, local copies, waits for them, and re-layouts, body(): whole_imag.astype(jnp.bfloat16)  14.2 us
    convert_element_type x2, local copies, waits for them, and re-layouts, body(): whole_real.astype(jnp.bfloat16)  14.2 us
    all_to_all x1, waiting for transfers between devices, body(): lax.all_to_all(projected, ROW, split_axis=1, concat_axis=0, tiled=True)  14.1 us
    all_to_all x1, starting transfers between devices, body(): lax.all_to_all(whole_imag.astype(jnp.bfloat16), ROW, split_axis=0, concat...  12.7 us
    all_to_all x1, blocking collectives, turned_gather(): lax.all_to_all(jnp.stack([both] * lax.axis_size(axis)), axis, 0, 0)  12.4 us
    dot_general x6, matrix products, table_dot(): return jnp.dot(matrix, values, preferred_element_type=jnp.float32)  11.7 us
  transfers between devices with their start and end apart: 5, of which 3 were waited for; matrix products, arithmetic and copies ran while one was open for 25% of the time, Pallas kernels for 0%

profile of v1, /device:TPU:2, one launch (start us, length us, event | category | flops | bytes accessed | tf_op | source)
XLA Modules:
  0.0 208.9 jit_solution(13310759961792153163)
XLA Ops:
  6.5 0.0 copy-start
  6.5 0.0 all-gather.7.cloned.1.call-start
  6.5 0.8 pad_maximum_fusion
  7.4 0.2 reshape.191
  7.6 12.4 %all_to_all.53 = bf16[8,2,2048]{2,1,0:T(2,128)(2,1)S(1)} all-to-all(bf16[8,2,2048]{2,1,0:T(2,128)(2,1)S(1)} %reshape.191), channel_id=1, replica_groups=mesh['row_0'=8,'row_1'=8,'col'=8] {'col'}, dimensions={0} | all-to-all | bytes 131072 | tf_op jit(solution)/shard_map/all_to_all | solution.py:18
  20.0 0.1 reshape.192
  20.1 0.1 copy.28
  20.2 0.1 reshape.183
  20.4 0.6 slice_bitcast_fusion
  21.0 29.6 %all-gather = bf16[256,512]{1,0:T(8,128)(2,1)} all-gather(bf16[32,512]{1,0:T(8,128)(2,1)S(1)} %get-tuple-element.7), channel_id=2, replica_groups=mesh['row_0'=8,'row_1'=8,'col'=8] {'row_0'}, dimensions={0}, use_global_device_ids=true | all-gather | bytes 294912 | tf_op jit(solution)/shard_map/all_gather | solution.py:38
  50.5 0.0 all-gather.7.cloned.1.call-update
  50.6 0.0 all-gather.5.cloned.1.call-start
  50.6 0.7 convert_element_type.78
  51.3 0.0 all-gather.5.cloned.1.call-update
  51.3 0.0 copy-done
  51.3 0.4 fusion
  51.7 39.6 %all-gather.7.cloned.1.call-done = bf16[64,32,512]{2,1,0:T(8,128)(2,1)} async-done(((bf16[8,32,512]{2,1,0:T(8,128)(2,1)}), bf16[64,32,512]{2,1,0:T(8,128)(2,1)}) %all-gather.7.cloned.1.call-update) | async-done | bytes 2097168 | tf_op jit(solution)/shard_map/all_gather | solution.py:38
  91.4 1.8 copy.29
  93.2 1.0 fusion.13
  94.2 0.9 copy.30
  95.2 10.7 %all-to-all-start.1 = ((bf16[384,64,8]{0,2,1:T(8,128)(2,1)}), bf16[384,64,8]{0,2,1:T(8,128)(2,1)S(1)}, u32[]{:S(2)}, u32[]{:S(2)}) async-start(bf16[384,64,8]{0,2,1:T(8,128)(2,1)} %bitcast.8), calls=%async_computation.1 | async-start | bytes 786432 | tf_op jit(solution)/shard_map/all_to_all | solution.py:85
  105.9 0.4 fusion.78
  106.3 14.1 %all-to-all-done.1 = bf16[384,64,8]{0,2,1:T(8,128)(2,1)S(1)} async-done(((bf16[384,64,8]{0,2,1:T(8,128)(2,1)}), bf16[384,64,8]{0,2,1:T(8,128)(2,1)S(1)}, u32[]{:S(2)}, u32[]{:S(2)}) %all-to-all-start.1) | async-done | bytes 393248 | tf_op jit(solution)/shard_map/all_to_all | solution.py:85
  120.4 0.6 copy.31
  121.1 0.5 convolution_negate_fusion
  121.5 0.5 copy.33
  122.0 0.5 copy.34
  122.6 0.5 subtract_bitcast_fusion
  123.0 2.5 %fusion.26 = f32[384,512]{1,0:T(8,128)S(1)} fusion(bf16[384,64,8]{0,1,2:T(8,128)(2,1)S(1)} %get-tuple-element.6), kind=kOutput, calls=%fused_computation.38 | convolution fusion | flops 152322048 | bytes 1179648 | tf_op jit(solution)/shard_map/dot_general | solution.py:56
  125.5 2.9 %fusion.10 = bf16[384,512]{1,0:T(8,128)(2,1)S(1)} fusion(f32[384,512]{1,0:T(8,128)S(1)} %fusion.26, bf16[384,64,8]{0,1,2:T(8,128)(2,1)S(1)} %get-tuple-element.5), kind=kOutput, calls=%fused_computation.23 | convolution fusion | flops 152715264 | bytes 1572864 | tf_op jit(solution)/shard_map/dot_general | solution.py:56
  128.4 8.4 %convert_element_type.84 = bf16[64,384,8]{2,1,0:T(8,128)(2,1)} reshape(bf16[384,512]{1,0:T(8,128)(2,1)S(1)} %fusion.10) | data formatting | bytes 786432 | tf_op jit(solution)/shard_map/convert_element_type | solution.py:107
  136.8 5.8 %copy.38 = bf16[64,384,8]{1,2,0:T(8,128)(2,1)} copy(bf16[64,384,8]{2,1,0:T(8,128)(2,1)} %convert_element_type.84) | data formatting | bytes 786432 | tf_op jit(solution)/shard_map/convert_element_type | solution.py:107
  142.6 4.8 %all-to-all-start.2 = ((bf16[64,384,8]{1,2,0:T(8,128)(2,1)}), bf16[64,384,8]{1,2,0:T(8,128)(2,1)S(1)}, u32[]{:S(2)}, u32[]{:S(2)}) async-start(bf16[64,384,8]{1,2,0:T(8,128)(2,1)} %copy.38), calls=%async_computation.2 | async-start | bytes 786432 | tf_op jit(solution)/shard_map/all_to_all | solution.py:106
  147.4 2.5 %fusion.22 = f32[384,512]{1,0:T(8,128)S(1)} fusion(bf16[384,64,8]{0,1,2:T(8,128)(2,1)S(1)} %get-tuple-element.5), kind=kOutput, calls=%fused_computation.34 | convolution fusion | flops 152322048 | bytes 1179648 | tf_op jit(solution)/shard_map/dot_general | solution.py:56
  150.0 2.9 %fusion.11 = bf16[384,512]{1,0:T(8,128)(2,1)S(1)} fusion(f32[384,512]{1,0:T(8,128)S(1)} %fusion.22, bf16[384,64,8]{0,1,2:T(8,128)(2,1)S(1)} %get-tuple-element.6), kind=kOutput, calls=%fused_computation.24 | convolution fusion | flops 152715264 | bytes 1572864 | tf_op jit(solution)/shard_map/dot_general | solution.py:56
  152.8 8.4 %convert_element_type.87 = bf16[64,384,8]{2,1,0:T(8,128)(2,1)} reshape(bf16[384,512]{1,0:T(8,128)(2,1)S(1)} %fusion.11) | data formatting | bytes 786432 | tf_op jit(solution)/shard_map/convert_element_type | solution.py:110
  161.2 5.8 %copy.39 = bf16[64,384,8]{1,2,0:T(8,128)(2,1)} copy(bf16[64,384,8]{2,1,0:T(8,128)(2,1)} %convert_element_type.87) | data formatting | bytes 786432 | tf_op jit(solution)/shard_map/convert_element_type | solution.py:110
  167.1 0.0 all-to-all-done.2
  167.1 12.7 %all-to-all-start.3 = ((bf16[64,384,8]{1,2,0:T(8,128)(2,1)}), bf16[64,384,8]{1,2,0:T(8,128)(2,1)S(1)}, u32[]{:S(2)}, u32[]{:S(2)}) async-start(bf16[64,384,8]{1,2,0:T(8,128)(2,1)} %copy.39), calls=%async_computation.3 | async-start | bytes 786432 | tf_op jit(solution)/shard_map/all_to_all | solution.py:109
  179.8 4.2 %fusion.16 = f32[384,512]{1,0:T(8,128)S(1)} fusion(s32[512]{0:T(512)S(1)} %get-tuple-element.11, s32[512]{0:T(512)S(1)} %get-tuple-element.12, bf16[64,384,8]{1,2,0:T(8,128)(2,1)S(1)} %all-to-all-done.2), kind=kOutput, calls=%fused_computation.27 | convolution fusion | flops 205520896 | bytes 1183744 | tf_op jit(solution)/shard_map/dot_general | solution.py:60
  183.9 0.0 all-gather.5.cloned.1.call-done
  184.0 10.3 %all-to-all-done.3 = bf16[64,384,8]{1,2,0:T(8,128)(2,1)S(1)} async-done(((bf16[64,384,8]{1,2,0:T(8,128)(2,1)}), bf16[64,384,8]{1,2,0:T(8,128)(2,1)S(1)}, u32[]{:S(2)}, u32[]{:S(2)}) %all-to-all-start.3) | async-done | bytes 393248 | tf_op jit(solution)/shard_map/all_to_all | solution.py:109
  194.3 7.8 %fusion.3 = bf16[1,384,2048]{2,1,0:T(8,128)(2,1)} fusion(bf16[512,2048]{0,1:T(8,128)(2,1)} %all-gather.5.cloned.1.call-done, f32[384,512]{1,0:T(8,128)S(1)} %fusion.16, s32[512]{0:T(512)S(1)} %get-tuple-element.11, s32[512]{0:T(512)S(1)} %get-tuple-element.12, bf16[64,384,8]{1,2,0:T(8,128)(2,1)S(1)} %all-to-all-done.3), kind=kOutput, calls=%fused_computation.7 | convolution fusion | flops 1012203520 | bytes 4853760 | tf_op jit(solution)/shard_map/dot_general | solution.py:115
  (3 shorter events, 0.0 us)
Async XLA Ops:
  6.5 44.8 %copy-start = (bf16[1,384,2048]{2,1,0:T(8,128)(2,1)S(1)}, bf16[1,384,2048]{2,1,0:T(8,128)(2,1)}, u32[]{:S(2)}) copy-start(bf16[1,384,2048]{2,1,0:T(8,128)(2,1)} %param.4) | copy-start | bytes 4718596
  6.5 84.8 %all-gather.7.cloned.1.call-start = ((), (), s32[]{:S(2)}) async-start(), calls=%async_computation.5 | async-start | bytes 2359296 | tf_op jit(solution)/shard_map/all_gather | solution.py:38
  50.6 133.4 %all-gather.5.cloned.1.call-start = ((), (), s32[]{:S(2)}) async-start(), calls=%async_computation.4 | async-start | bytes 2129920 | tf_op jit(solution)/shard_map/all_gather | solution.py:117
  95.2 25.3 %all-to-all-start.1 = ((bf16[384,64,8]{0,2,1:T(8,128)(2,1)}), bf16[384,64,8]{0,2,1:T(8,128)(2,1)S(1)}, u32[]{:S(2)}, u32[]{:S(2)}) async-start(bf16[384,64,8]{0,2,1:T(8,128)(2,1)} %bitcast.8), calls=%async_computation.1 | async-start | bytes 786432 | tf_op jit(solution)/shard_map/all_to_all | solution.py:85
  142.6 24.4 %all-to-all-start.2 = ((bf16[64,384,8]{1,2,0:T(8,128)(2,1)}), bf16[64,384,8]{1,2,0:T(8,128)(2,1)S(1)}, u32[]{:S(2)}, u32[]{:S(2)}) async-start(bf16[64,384,8]{1,2,0:T(8,128)(2,1)} %copy.38), calls=%async_computation.2 | async-start | bytes 786432 | tf_op jit(solution)/shard_map/all_to_all | solution.py:106
  167.1 27.3 %all-to-all-start.3 = ((bf16[64,384,8]{1,2,0:T(8,128)(2,1)}), bf16[64,384,8]{1,2,0:T(8,128)(2,1)S(1)}, u32[]{:S(2)}, u32[]{:S(2)}) async-start(bf16[64,384,8]{1,2,0:T(8,128)(2,1)} %copy.39), calls=%async_computation.3 | async-start | bytes 786432 | tf_op jit(solution)/shard_map/all_to_all | solution.py:109
Sparse Core Ops, SparseCore 0:
  50.7 40.6 all-gather.6
  94.4 85.9 all-gather.4
